TPU v7x, 32 devices: a whole 2x2x4 slice. The times are simulated.
32 devices in a mesh: sp: 16 (over z, y, x), tp: 2 (over core).
Axes of the slice: x: 2, y: 2, z: 4, core: 2. Of those that a mesh axis runs over, the one named last changes fastest.
Arguments:
- queries: bfloat16 [4096, 1024], P('sp', 'tp'), may hold values from -12 to 12
- keys: bfloat16 [4096, 1024], P('sp', 'tp'), may hold values from -6 to 6
- values: bfloat16 [4096, 1024], P('sp', 'tp'), may hold values from -6 to 6
- w_out: bfloat16 [1024, 2048], P(None, 'tp'), may hold values from -0.375 to 0.375
Outputs:
- mixed: bfloat16 [4096, 2048], P('sp', 'tp')
All inputs are finite; a program needn't handle non-finite values.
Results may differ from a plain program's by a relative error of at most 0.0056.
Values may be sent and summed in bfloat16 or wider, within the bound.
A program may use at most 64 MiB of HBM per device.

v0:
```python
import functools
import math

import jax
import jax.numpy as jnp
from jax import lax
from jax.experimental import pallas as pl
from jax.experimental.pallas import tpu as pltpu
from jax.sharding import PartitionSpec as P

HEAD_DIM = 128
SIDE = 64
MID = 4
FAR = 16
MESH = pl.DeviceIdType.MESH
F32 = jnp.float32
BF16 = jnp.bfloat16
SCALE = HEAD_DIM ** -0.5 * math.log2(math.e)


def nt(a, b):
    return lax.dot_general(a, b, (((1,), (1,)), ((), ())), preferred_element_type=F32)


def nn(a, b):
    return lax.dot_general(a, b, (((1,), (0,)), ((), ())), preferred_element_type=F32)


def iota(shape, dim):
    return lax.broadcasted_iota(jnp.int32, shape, dim)


def attend(q, k, v, allowed):
    s = jnp.where(allowed, nt(q, k) * SCALE, -jnp.inf)
    top = jnp.max(s, axis=-1, keepdims=True)
    raised = jnp.exp2(s - top)
    den = jnp.sum(raised, axis=-1, keepdims=True)
    return nn(raised.astype(BF16), v), top, den


def kernel(sp_n, heads, q_hbm, k_hbm, v_hbm, out_ref,
           q_in, k_in, v_in, pkv, kvf, near_lo, near_hi, ob, ret, att, att_other, acc_n, md_n,
           relay, load_sem, hop_s, hop_r, kv_s, kv_r, q_s, q_r, up_s, up_r, dn_s, dn_r, near_s, near_r, ret_s, ret_r, tp_s, tp_r):
    rows = q_in.shape[0]
    chunk = rows // MID
    mm = rows // FAR
    e = HEAD_DIM
    p, c = lax.axis_index("sp"), lax.axis_index("tp")
    groups = sp_n // MID
    g, j = p // MID, p % MID

    loads = [
        pltpu.make_async_copy(src, dst, load_sem.at[n])
        for n, (src, dst) in enumerate(((k_hbm, k_in), (v_hbm, v_in), (q_hbm, q_in)))
    ]
    for load in loads:
        load.start()

    barrier = pltpu.get_barrier_semaphore()

    def greet(sp, tp):
        pl.semaphore_signal(barrier, inc=1, device_id=(sp, tp), device_id_type=MESH)

    def mate(d):
        return g * MID + (j + d) % MID

    for d in range(1, MID):
        greet(mate(d), c)
    greet(p, 1 - c)
    has_dn, has_up = g > 0, g < groups - 1
    has_prev, has_next = p > 0, p < sp_n - 1

    @pl.when(has_dn)
    def _():
        greet(p - MID, c)

    @pl.when(has_up)
    def _():
        greet(p + MID, c)

    @pl.when(has_prev)
    def _():
        greet(p - 1, c)

    @pl.when(has_next)
    def _():
        greet(p + 1, c)

    def remote(src, dst, ss, rs, sp, tp):
        return pltpu.make_async_remote_copy(
            src_ref=src, dst_ref=dst, send_sem=ss, recv_sem=rs, device_id=(sp, tp), device_id_type=MESH)

    r, t = iota((rows, rows), 0), iota((rows, rows), 1)
    perm = (t == FAR * (r % mm) + MID * ((r % chunk) // mm) + r // chunk).astype(BF16)
    r, t = t, r
    back = (t == FAR * (r % mm) + MID * ((r % chunk) // mm) + r // chunk).astype(BF16)

    for n, x in enumerate((k_in, v_in, q_in)):
        loads[n].wait()
        moved = nn(perm, x[...]).astype(BF16)
        for h in range(heads):
            pkv[h, n] = moved[:, h * e:(h + 1) * e]

    def at(n, base=0):
        return pl.ds(pl.multiple_of(base + n * chunk, chunk), chunk)

    for h in range(heads):
        for n in range(3):
            kvf[h, n, at(j, rows), :] = pkv[h, n, at(j), :]

    def edge(test, rows_at):
        @pl.when(jnp.logical_not(test))
        def _():
            for h in range(heads):
                for n in range(2):
                    kvf[h, n, pl.ds(rows_at, rows), :] = jnp.zeros((rows, e), BF16)

    edge(has_dn, 0)
    edge(has_up, 2 * rows)

    @pl.when(jnp.logical_not(has_prev))
    def _():
        near_lo[...] = jnp.zeros_like(near_lo)

    @pl.when(jnp.logical_not(has_next))
    def _():
        near_hi[...] = jnp.zeros_like(near_hi)

    pl.semaphore_wait(
        barrier,
        MID + has_dn.astype(jnp.int32) + has_up.astype(jnp.int32)
        + has_prev.astype(jnp.int32) + has_next.astype(jnp.int32))

    def up(h, d):
        n = (j - d + MID) % MID
        src = pkv.at[h, 0:2, at(n), :] if d == 0 else kvf.at[h, 0:2, at(n, rows), :]
        return remote(src, kvf.at[h, 0:2, at(n), :], up_s.at[h, d], up_r.at[h, d], (p + MID) % sp_n, c)

    def down(h, d):
        n = (j - d + MID) % MID
        src = pkv.at[h, 0:2, at(n), :] if d == 0 else kvf.at[h, 0:2, at(n, rows), :]
        return remote(src, kvf.at[h, 0:2, at(n, 2 * rows), :], dn_s.at[h, d], dn_r.at[h, d], (p - MID + sp_n) % sp_n, c)

    def forward(h, d):
        @pl.when(has_up)
        def _():
            up(h, d).start()

        @pl.when(has_dn)
        def _():
            down(h, d).start()

    def kv(h, d, receive=False):
        dst = (j - d + MID) % MID if receive else j
        return remote(pkv.at[h, 0:2, at((j + d) % MID), :], kvf.at[h, 0:2, at(dst, rows), :],
                      kv_s.at[h, d - 1], kv_r.at[h, d - 1], mate(d), c)

    def queries(d, receive=False):
        dst = (j - d + MID) % MID if receive else j
        return remote(pkv.at[:, 2, at((j + d) % MID), :], kvf.at[:, 2, at(dst, rows), :],
                      q_s.at[d - 1], q_r.at[d - 1], mate(d), c)

    for h in range(heads):
        for d in range(1, MID):
            kv(h, d).start()
        forward(h, 0)
    for d in range(1, MID):
        queries(d).start()

    def near(n, to_next):
        src = (k_in, v_in)[n]
        if to_next:
            return remote(src.at[pl.ds(rows - SIDE, SIDE), :], near_lo.at[n],
                          near_s.at[n, 0], near_r.at[n, 0], (p + 1) % sp_n, c)
        return remote(src.at[pl.ds(0, SIDE), :], near_hi.at[n],
                      near_s.at[n, 1], near_r.at[n, 1], (p - 1 + sp_n) % sp_n, c)

    def hop(side):
        first = (rows - SIDE, 0)[side]
        to = ((p + MID) % sp_n, (p - MID + sp_n) % sp_n)[side]
        return remote(v_in.at[pl.ds(first, SIDE), :], relay.at[side], near_s.at[1, side], hop_r.at[side], to, c)

    def pass_on(side):
        dst = (near_lo, near_hi)[side]
        return remote(relay.at[side], dst.at[1], hop_s.at[side], near_r.at[1, side], mate((1, MID - 1)[side]), c)

    @pl.when(has_next)
    def _():
        near(0, True).start()

    @pl.when(has_prev)
    def _():
        near(0, False).start()

    @pl.when(has_next & (j < MID - 1))
    def _():
        near(1, True).start()

    @pl.when(has_prev & (j > 0))
    def _():
        near(1, False).start()

    @pl.when(has_up & (j == MID - 1))
    def _():
        hop(0).start()

    @pl.when(has_dn & (j == 0))
    def _():
        hop(1).start()

    half = rows // 2
    own_span = half + SIDE
    qi, ki = iota((half, own_span), 0), iota((half, own_span), 1)
    for b in range(2):
        at_q = slice(b * half, (b + 1) * half)
        at_k = slice(b * (half - SIDE), b * (half - SIDE) + own_span)
        gap = (ki + at_k.start) - (qi + at_q.start)
        near_ok = (gap >= -SIDE) & (gap <= SIDE)
        for h in range(heads):
            cols = slice(h * e, (h + 1) * e)
            o, top, den = attend(q_in[at_q, cols], k_in[at_k, cols], v_in[at_k, cols], near_ok)
            acc_n[h, at_q, :] = o
            md_n[h, 0, at_q, :] = jnp.broadcast_to(top, (half, e))
            md_n[h, 1, at_q, :] = jnp.broadcast_to(den, (half, e))

    for h in range(heads):
        for d in range(1, MID):
            kv(h, d, receive=True).wait_recv()
            forward(h, d)

    relays = (has_dn & (j == MID - 1), has_up & (j == 0))
    for side in range(2):
        @pl.when(relays[side])
        def _():
            hop(side).wait_recv()
            pass_on(side).start()

    span = half + 2 * SIDE
    qi, ki = iota((half, span), 0), iota((half, span), 1)

    def order(x):
        return chunk * (x // chunk) + (FAR // MID) * (x % mm) + (x % chunk) // mm

    dn_ok, up_ok = has_dn.astype(jnp.int32), has_up.astype(jnp.int32)
    gap = order(ki) - order(qi)
    band = (gap >= 0) & (gap <= 2 * SIDE)
    mid_ok = (band & ((ki >= SIDE) | (dn_ok == 1)), band & ((ki < span - SIDE) | (up_ok == 1)))
    far_span, ns = 4 * chunk, FAR // MID
    ones = jnp.ones((far_span, e), BF16)
    qi, ki = iota((chunk, far_span), 0), iota((chunk, far_span), 1)
    far_ok = ((ki >= qi) & (ki <= qi + 2 * SIDE) & ((ki >= chunk) | (dn_ok == 1))
              & ((ki < 2 * chunk) | (up_ok == 1)))
    lane = iota((rows, e), 1)
    for d in range(1, MID):
        queries(d, receive=True).wait_recv()
    pick = (iota((16, e), 0) == iota((16, e), 1)).astype(BF16)

    def result(h, d, receive=False):
        dst = (j - d + MID) % MID if receive else j
        return remote(ob.at[h, (j + d) % MID], ret.at[h, dst],
                      ret_s.at[h, d - 1], ret_r.at[h, d - 1], mate(d), c)

    for h in range(heads):
        @pl.when(has_dn)
        def _():
            for d in range(MID):
                up(h, d).wait_recv()

        @pl.when(has_up)
        def _():
            for d in range(MID):
                down(h, d).wait_recv()

        q = kvf[h, 2, pl.ds(rows, rows), :]
        kh, vh = kvf[h, 0], kvf[h, 1]
        firsts = [rows - chunk + b * half for b in range(2)]
        s_mid = jnp.concatenate([
            jnp.where(mid_ok[b], nt(q[b * half:(b + 1) * half], kh[f:f + span]), -jnp.inf)
            for b, f in enumerate(firsts)], axis=0)
        q4 = q.reshape(MID, ns, mm, e)

        def classes(x):
            x4 = x.reshape(3 * MID, ns, mm, e)
            return [jnp.concatenate([x4[:, n], x4[:MID, n]], axis=0).reshape(far_span, e) for n in range(ns)]

        k_far, v_far = classes(kh), classes(vh)
        far = [jnp.where(far_ok, nt(q4[:, n].reshape(chunk, e), k_far[n]), -jnp.inf) for n in range(ns)]
        s_far = jnp.concatenate([far[n][i * mm:(i + 1) * mm] for i in range(MID) for n in range(ns)], axis=0)
        peak = functools.reduce(
            jnp.maximum, [x[:, i:i + e] for x in (s_mid, s_far) for i in range(0, x.shape[1], e)])
        top = jnp.max(peak, axis=-1, keepdims=True)
        r_mid = jnp.exp2((s_mid - top) * SCALE).astype(BF16)
        r_far = jnp.exp2((s_far - top) * SCALE).astype(BF16)
        total = jnp.concatenate([
            nn(r_mid[b * half:(b + 1) * half], jnp.concatenate([vh[f:f + span], ones], axis=1))
            for b, f in enumerate(firsts)], axis=0)
        far = [
            nn(jnp.concatenate([r_far[(i * ns + n) * mm:(i * ns + n + 1) * mm] for i in range(MID)], axis=0),
               jnp.concatenate([v_far[n], ones], axis=1))
            for n in range(ns)]
        total += jnp.concatenate([far[n][i * mm:(i + 1) * mm] for i in range(MID) for n in range(ns)], axis=0)
        den = total[:, e:]
        o = (total[:, :e] / den).astype(BF16)
        log_den = top * SCALE + jnp.log2(den)
        one = log_den.astype(BF16).astype(F32)
        two = (log_den - one).astype(BF16).astype(F32)
        three = log_den - one - two
        parts = jnp.where(lane == 0, one, jnp.where(lane == 1, two, three)).astype(BF16)
        twice = [parts[i * chunk:(i + 1) * chunk] for i in range(MID) for _ in range(2)]
        flat = nt(pick, jnp.concatenate(twice, axis=0)).astype(BF16)
        for i in range(MID):
            ob[h, i, :chunk] = o[i * chunk:(i + 1) * chunk]
            ob[h, i, chunk:] = flat[:, 2 * i * chunk:2 * (i + 1) * chunk]
        for d in range(1, MID):
            result(h, d).start()
        ret[h, pl.ds(j, 1)] = ob[h, pl.ds(j, 1)]

    @pl.when(has_prev)
    def _():
        for n in range(2):
            near(n, True).wait_recv()

    @pl.when(has_next)
    def _():
        for n in range(2):
            near(n, False).wait_recv()

    lo_ok, hi_ok = has_prev.astype(jnp.int32), has_next.astype(jnp.int32)
    qi, ki = iota((SIDE, SIDE), 0), iota((SIDE, SIDE), 1)
    corners = (
        (near_lo, slice(0, SIDE), (ki >= qi) & (lo_ok == 1)),
        (near_hi, slice(rows - SIDE, rows), (ki <= qi) & (hi_ok == 1)),
    )
    for h in range(heads):
        cols = slice(h * e, (h + 1) * e)
        for halo, at_q, ok in corners:
            s = jnp.where(ok, nt(q_in[at_q, cols], halo[0, :, cols]) * SCALE, -jnp.inf)
            old = md_n[h, 0, at_q, :]
            top = jnp.maximum(old, jnp.max(s, axis=-1, keepdims=True))
            fade = jnp.exp2(old - top)
            raised = jnp.exp2(s - top[:, :SIDE])
            acc_n[h, at_q, :] = fade * acc_n[h, at_q, :] + nn(raised.astype(BF16), halo[1, :, cols])
            md_n[h, 0, at_q, :] = top
            md_n[h, 1, at_q, :] = fade * md_n[h, 1, at_q, :] + jnp.sum(raised, axis=-1, keepdims=True)

    r, t = iota((rows, 2 * rows), 1), iota((rows, 2 * rows), 0)
    low = r % (2 * chunk) < chunk
    r = r // (2 * chunk) * chunk + r % (2 * chunk)
    back_twice = (low & (t == FAR * (r % mm) + MID * ((r % chunk) // mm) + r // chunk)).astype(BF16)

    def share(h):
        cols = pl.ds(h * e, e)
        return remote(att.at[:, cols], att_other.at[:, cols], tp_s.at[h], tp_r.at[h], p, 1 - c)

    for h in range(heads):
        for d in range(1, MID):
            result(h, d, receive=True).wait_recv()
        o = nn(back, jnp.concatenate([ret[h, i, :chunk] for i in range(MID)], axis=0))
        parts = nt(back_twice, jnp.concatenate([ret[h, i, chunk:] for i in range(MID)], axis=1))
        log_den = parts[:, 0:1] + parts[:, 1:2] + parts[:, 2:3]
        t_n, d_n = md_n[h, 0], md_n[h, 1]
        top = jnp.maximum(t_n, log_den)
        e1, e2 = jnp.exp2(t_n - top), jnp.exp2(log_den - top)
        att[:, h * e:(h + 1) * e] = ((e1 * acc_n[h] + e2 * o) / (e1 * d_n + e2)).astype(BF16)
        share(h).start()

    width = heads * e
    out_ref[:, pl.ds(pl.multiple_of(c * width, width), width)] = att[...]
    for h in range(heads):
        share(h).wait_recv()
        out_ref[:, pl.ds(pl.multiple_of((1 - c) * width + h * e, e), e)] = att_other[:, h * e:(h + 1) * e]

    for h in range(heads):
        for d in range(1, MID):
            kv(h, d).wait_send()
            result(h, d).wait_send()
        share(h).wait_send()
    for d in range(1, MID):
        queries(d).wait_send()
    for side in range(2):
        @pl.when(relays[side])
        def _():
            pass_on(side).wait_send()
    @pl.when(has_up)
    def _():
        for h in range(heads):
            for d in range(MID):
                up(h, d).wait_send()

    @pl.when(has_dn)
    def _():
        for h in range(heads):
            for d in range(MID):
                down(h, d).wait_send()

    @pl.when(has_next)
    def _():
        for n in range(2):
            near(n, True).wait_send()

    @pl.when(has_prev)
    def _():
        for n in range(2):
            near(n, False).wait_send()


def per_device(sp_n, q, k, v, w):
    rows, columns = q.shape
    heads = columns // HEAD_DIM
    assert MID * rows == SIDE * FAR and rows // MID == SIDE and sp_n % MID == 0
    dma = pltpu.SemaphoreType.DMA
    e, chunk = HEAD_DIM, rows // MID
    attended = pl.pallas_call(
        functools.partial(kernel, sp_n, heads),
        out_shape=jax.ShapeDtypeStruct((rows, w.shape[0]), BF16),
        in_specs=[pl.BlockSpec(memory_space=pl.ANY)] * 3,
        out_specs=pl.BlockSpec(memory_space=pltpu.VMEM),
        scratch_shapes=[
            pltpu.VMEM((rows, columns), BF16),
            pltpu.VMEM((rows, columns), BF16),
            pltpu.VMEM((rows, columns), BF16),
            pltpu.VMEM((heads, 3, rows, e), BF16),
            pltpu.VMEM((heads, 3, 3 * rows, e), BF16),
            pltpu.VMEM((2, SIDE, columns), BF16),
            pltpu.VMEM((2, SIDE, columns), BF16),
            pltpu.VMEM((heads, MID, chunk + 16, e), BF16),
            pltpu.VMEM((heads, MID, chunk + 16, e), BF16),
            pltpu.VMEM((rows, columns), BF16),
            pltpu.VMEM((rows, columns), BF16),
            pltpu.VMEM((heads, rows, e), F32),
            pltpu.VMEM((heads, 2, rows, e), F32),
            pltpu.VMEM((2, SIDE, columns), BF16),
            dma((3,)),
            dma((2,)), dma((2,)),
            dma((heads, MID - 1)), dma((heads, MID - 1)),
            dma((MID - 1,)), dma((MID - 1,)),
            dma((heads, MID)), dma((heads, MID)),
            dma((heads, MID)), dma((heads, MID)),
            dma((2, 2)), dma((2, 2)),
            dma((heads, MID - 1)), dma((heads, MID - 1)),
            dma((heads,)), dma((heads,)),
        ],
        compiler_params=pltpu.CompilerParams(collective_id=0, has_side_effects=True),
    )(q, k, v)
    return nn(attended, w).astype(BF16)


def solution(mesh):
    return jax.shard_map(
        functools.partial(per_device, mesh.shape["sp"]), mesh=mesh,
        in_specs=(P("sp", "tp"), P("sp", "tp"), P("sp", "tp"), P(None, "tp")),
        out_specs=P("sp", "tp"), check_vma=False,
    )
```

profile of v0, /device:TPU:1, one launch (start us, length us, event | category | flops | bytes accessed | tf_op | source)
XLA Modules:
  0.0 29.8 jit_solution(2099319537296044539)
XLA Ops:
  0.0 0.0 copy-start
  0.0 27.2 %shard_map.46 = bf16[256,1024]{1,0:T(8,128)(2,1)} custom-call(bf16[256,512]{1,0:T(8,128)(2,1)} %q_hbm.1, bf16[256,512]{1,0:T(8,128)(2,1)} %k_hbm.1, bf16[256,512]{1,0:T(8,128)(2,1)} %v_hbm.1), custom_call_target="tpu_custom_call" | custom-call | tf_op jit(solution)/shard_map/pallas_call | solution.py:413
  27.2 0.0 copy-done
  27.2 2.5 %convolution_convert_fusion = bf16[256,1024]{1,0:T(8,128)(2,1)} fusion(bf16[256,1024]{1,0:T(8,128)(2,1)} %shard_map.46, bf16[1024,1024]{1,0:T(8,128)(2,1)S(1)} %copy-done), kind=kOutput, calls=%fused_computation | convolution fusion | flops 537133056 | bytes 3145728 | tf_op jit(solution)/shard_map/dot_general | solution.py:26
Async XLA Ops:
  0.0 27.2 %copy-start = (bf16[1024,1024]{1,0:T(8,128)(2,1)S(1)}, bf16[1024,1024]{1,0:T(8,128)(2,1)}, u32[]{:S(2)}) copy-start(bf16[1024,1024]{1,0:T(8,128)(2,1)} %param.7) | copy-start | bytes 6291460
where the time goes:
time: 30 us; the launch traced here: 29.8 us
  Pallas kernels  27.2 us (91%)
  matrix products  2.55 us (8%)
    pallas_call x1, Pallas kernels, per_device(): pl.pallas_call(functools.partial(kernel, sp_n, heads), out_shape=jax.Shap...  27.2 us
    dot_general x1, matrix products, nn(): lax.dot_general(a, b, (((1,), (0,)), ((), ())), preferred_element_type=F32)  2.55 us

commit v1 on v0

--- a/solution.py
+++ b/solution.py
@@ -412,8 +412,8 @@
     e, chunk = HEAD_DIM, rows // MID
     attended = pl.pallas_call(
         functools.partial(kernel, sp_n, heads),
-        out_shape=jax.ShapeDtypeStruct((rows, w.shape[0]), BF16),
-        in_specs=[pl.BlockSpec(memory_space=pl.ANY)] * 3,
+        out_shape=pltpu.VMEM((rows, w.shape[0]), BF16),
+        in_specs=[pl.BlockSpec(memory_space=pltpu.HBM)] * 3,
         out_specs=pl.BlockSpec(memory_space=pltpu.VMEM),
         scratch_shapes=[
             pltpu.VMEM((rows, columns), BF16),
@@ -440,8 +440,8 @@
             dma((heads, MID - 1)), dma((heads, MID - 1)),
             dma((heads,)), dma((heads,)),
         ],
-        compiler_params=pltpu.CompilerParams(collective_id=0, has_side_effects=True),
-    )(q, k, v)
+        compiler_params=pltpu.CompilerParams(collective_id=0, has_side_effects=True, vmem_limit_bytes=40*1024*1024),
+    )(*[pltpu.with_memory_space_constraint(x, pltpu.HBM) for x in (q, k, v)])
     return nn(attended, w).astype(BF16)
 
 

time: 30 us -> 28.2 us (0.940)
  matrix products: 2.55 us -> 1.51 us
  Pallas kernels: 27.2 us -> 26.4 us
    dot_general x1, matrix products: 2.55 us -> 1.51 us  [nn(): lax.dot_general(a, b, (((1,), (0,)), ((), ())), preferred_element_type=F32)]
    pallas_call x1, Pallas kernels: 27.2 us -> 26.4 us  [per_device(): pl.pallas_call(functools.partial(kernel, sp_n, heads), out_shape=pltpu.VM...]
where the time goes in v1:
time: 28.2 us; the launch traced here: 28 us
  Pallas kernels  26.4 us (94%)
  matrix products  1.51 us (5%)
    pallas_call x1, Pallas kernels, per_device(): pl.pallas_call(functools.partial(kernel, sp_n, heads), out_shape=pltpu.VM...  26.4 us
    dot_general x1, matrix products, nn(): lax.dot_general(a, b, (((1,), (0,)), ((), ())), preferred_element_type=F32)  1.51 us

profile of v1, /device:TPU:1, one launch (start us, length us, event | category | flops | bytes accessed | tf_op | source)
XLA Modules:
  0.0 28.0 jit_solution(2954161070485689722)
XLA Ops:
  0.0 0.0 copy-start
  0.0 26.4 %shard_map.46 = bf16[256,1024]{1,0:T(8,128)(2,1)S(1)} custom-call(bf16[256,512]{1,0:T(8,128)(2,1)} %q_hbm.1, bf16[256,512]{1,0:T(8,128)(2,1)} %k_hbm.1, bf16[256,512]{1,0:T(8,128)(2,1)} %v_hbm.1), custom_call_target="tpu_custom_call" | custom-call | tf_op jit(solution)/shard_map/pallas_call | solution.py:413
  26.5 0.0 copy-done
  26.5 1.5 %convolution_convert_fusion = bf16[256,1024]{1,0:T(8,128)(2,1)} fusion(bf16[256,1024]{1,0:T(8,128)(2,1)S(1)} %shard_map.46, bf16[1024,1024]{1,0:T(8,128)(2,1)S(1)} %copy-done), kind=kOutput, calls=%fused_computation | convolution fusion | flops 537133056 | bytes 3145728 | tf_op jit(solution)/shard_map/dot_general | solution.py:26
Async XLA Ops:
  0.0 26.5 %copy-start = (bf16[1024,1024]{1,0:T(8,128)(2,1)S(1)}, bf16[1024,1024]{1,0:T(8,128)(2,1)}, u32[]{:S(2)}) copy-start(bf16[1024,1024]{1,0:T(8,128)(2,1)} %param.7) | copy-start | bytes 6291460

commit v2 on v1

v2 whole, which is shorter than its diff:
```python
import functools
import math

import jax
import jax.numpy as jnp
from jax import lax
from jax.experimental import pallas as pl
from jax.experimental.pallas import tpu as pltpu
from jax.sharding import PartitionSpec as P

HEAD_DIM = 128
SIDE = 64
MID = 4
FAR = 16
NS = FAR // MID
MESH = pl.DeviceIdType.MESH
F32 = jnp.float32
BF16 = jnp.bfloat16
SCALE = HEAD_DIM ** -0.5 * math.log2(math.e)
NEG = -jnp.inf


def nt(a, b):
    return lax.dot_general(a, b, (((1,), (1,)), ((), ())), preferred_element_type=F32)


def nn(a, b):
    return lax.dot_general(a, b, (((1,), (0,)), ((), ())), preferred_element_type=F32)


def iota(shape, dim):
    return lax.broadcasted_iota(jnp.int32, shape, dim)


def bias(ok):
    return jnp.where(ok, 0.0, NEG).astype(F32)


def kernel(sp_n, heads, q_hbm, k_hbm, v_hbm, w_hbm, out_ref,
           q_in, k_in, v_in, w_in, ps, kv, qp, edge_in, edge_out, ends, near_bias, mid_bias, far_bias, rim_bias,
           o_s, t_s, d_s, ob, att, ys,
           load_sem, kv_s, kv_r, q_s, q_r, up_s, up_r, dn_s, dn_r, ei_s, ei_r, eo_s, eo_r,
           res_s, res_r, cross_s, cross_r, tp_s, tp_r):
    rows = q_in.shape[0]
    chunk = rows // MID
    mm = rows // FAR
    e = HEAD_DIM
    width = heads * e
    last = MID - 1
    p, c = lax.axis_index("sp"), lax.axis_index("tp")
    groups = sp_n // MID
    g, j = p // MID, p % MID

    loads = [
        pltpu.make_async_copy(src, dst, load_sem.at[n])
        for n, (src, dst) in enumerate(((k_hbm, k_in), (v_hbm, v_in), (q_hbm, q_in), (w_hbm, w_in)))
    ]
    for load in loads:
        load.start()

    barrier = pltpu.get_barrier_semaphore()

    def greet(sp, tp):
        pl.semaphore_signal(barrier, inc=1, device_id=(sp, tp), device_id_type=MESH)

    def mate(d):
        return g * MID + (j + d) % MID

    for d in range(1, MID):
        greet(mate(d), c)
        greet(mate(d), 1 - c)
    greet(p, 1 - c)
    has_dn, has_up = g > 0, g < groups - 1

    @pl.when(has_dn)
    def _():
        greet(p - MID, c)

    @pl.when(has_up)
    def _():
        greet(p + MID, c)

    def remote(src, dst, ss, rs, sp, tp):
        return pltpu.make_async_remote_copy(
            src_ref=src, dst_ref=dst, send_sem=ss, recv_sem=rs, device_id=(sp, tp), device_id_type=MESH)

    def token(r):
        return FAR * (r % mm) + MID * ((r % chunk) // mm) + r // chunk

    r, t = iota((rows, rows), 0), iota((rows, rows), 1)
    perm = (t == token(r)).astype(BF16)
    back = (r == token(t)).astype(BF16)

    for n, x in enumerate((k_in, v_in, q_in)):
        loads[n].wait()
        moved = nn(perm, x[...]).astype(BF16)
        for h in range(heads):
            for m in range(MID):
                ps[m, h, n] = moved[m * chunk:(m + 1) * chunk, h * e:(h + 1) * e]

    up_p, dn_p = (p + MID) % sp_n, (p - MID + sp_n) % sp_n
    has = (has_up, has_dn)

    @pl.when(jnp.logical_not(has_dn))
    def _():
        kv[0] = jnp.zeros(kv.shape[1:], BF16)
        edge_out[0] = jnp.zeros(edge_out.shape[1:], BF16)

    @pl.when(jnp.logical_not(has_up))
    def _():
        kv[2] = jnp.zeros(kv.shape[1:], BF16)
        edge_out[1] = jnp.zeros(edge_out.shape[1:], BF16)

    pl.semaphore_wait(barrier, 2 * MID - 1 + has_dn.astype(jnp.int32) + has_up.astype(jnp.int32))

    def give(m, d, receive=False):
        dst = (j - d + MID) % MID if receive else j
        return remote(ps.at[m, (j + d) % MID, pl.ds(0, 2)], kv.at[1, m, :, dst],
                      kv_s.at[m, d - 1], kv_r.at[m, d - 1], mate(d), c)

    def ask(i, d, receive=False):
        dst = (j - d + MID) % MID if receive else j
        two = pl.ds(2 * i, 2)
        return remote(ps.at[two, (j + d) % MID, 2], qp.at[two, dst],
                      q_s.at[i, d - 1], q_r.at[i, d - 1], mate(d), c)

    def up(m, d):
        n = (j - d + MID) % MID
        src = ps.at[m, j, pl.ds(0, 2)] if d == 0 else kv.at[1, m, :, n]
        return remote(src, kv.at[0, m, :, n], up_s.at[m, d], up_r.at[m, d], up_p, c)

    def down(m, d):
        n = (j - d + MID) % MID
        src = ps.at[m, j, pl.ds(0, 2)] if d == 0 else kv.at[1, m, :, n]
        return remote(src, kv.at[2, m, :, n], dn_s.at[m, d], dn_r.at[m, d], dn_p, c)

    def forward(m, d):
        @pl.when(has_up)
        def _():
            up(m, d).start()

        @pl.when(has_dn)
        def _():
            down(m, d).start()

    homes = (j == last, j == 0)
    firsts = (rows - SIDE, 0)
    out_p = (up_p, dn_p)

    def rim_in(side, n, d):
        src = (k_in, v_in)[n].at[pl.ds(firsts[side], SIDE), pl.ds(pl.multiple_of((j + d) % MID * e, e), e)]
        return remote(src, edge_in.at[side, n], ei_s.at[side, n, d - 1], ei_r.at[side, n], mate(d), c)

    def rim_out(side, n, home):
        src = (k_in, v_in)[n].at[pl.ds(firsts[side], SIDE), pl.ds(pl.multiple_of(j * e, e), e)] if home else edge_in.at[side, n]
        return remote(src, edge_out.at[side, n], eo_s.at[side, n], eo_r.at[side, n], out_p[side], c)

    def give_all(m):
        for d in range(1, MID):
            give(m, d).start()

    def ask_all(i):
        for d in range(1, MID):
            ask(i, d).start()

    give_all(0)
    for m in range(MID):
        forward(m, 0)
    give_all(1)
    for side in range(2):
        @pl.when(has[side] & homes[side])
        def _():
            for n in range(2):
                for d in range(1, MID):
                    rim_in(side, n, d).start()
                rim_out(side, n, True).start()
    ask_all(0)
    give_all(2)
    give_all(3)
    ask_all(1)

    for m in range(MID):
        kv[1, m, :, pl.ds(j, 1)] = ps[m, pl.ds(j, 1), 0:2].reshape(2, 1, chunk, e)
        qp[m, pl.ds(j, 1)] = ps[m, pl.ds(j, 1), 2]

    ok_dn, ok_up = has_dn.astype(jnp.int32) == 1, has_up.astype(jnp.int32) == 1
    tq, s = token(iota((rows, rows), 0)), iota((rows, rows), 1)
    gap = tq - token(s)
    near_bias[:, :rows] = bias((gap >= -SIDE) & (gap <= SIDE))
    tq, s = token(iota((rows, 2 * SIDE), 0)), iota((rows, 2 * SIDE), 1)
    near_bias[:, rows:] = bias(((s < SIDE) & (s >= tq)) | ((s >= SIDE) & (s - SIDE <= tq - (rows - SIDE))))

    def order(x):
        return chunk * (x // chunk) + NS * (x % mm) + (x % chunk) // mm

    half = rows // 2
    uq, uk = order(iota((half, 3 * chunk), 0)), order(iota((half, 3 * chunk), 1))
    for i in range(2):
        gap = uk - uq - i * chunk
        mid_bias[i] = bias((gap >= -SIDE) & (gap <= SIDE))
    x, s = iota((chunk, 2 * chunk), 0), iota((chunk, 2 * chunk), 1)
    far_bias[...] = bias(((s < chunk) & (s >= x) & ok_dn) | ((s >= chunk) & (s - chunk <= x) & ok_up))
    x, s = iota((half, 2 * chunk), 0), iota((half, 2 * chunk), 1)
    u, v = order(x % chunk), order(s % chunk)
    rim_bias[...] = bias(((x < chunk) & (s < chunk) & (v >= u) & ok_dn)
                         | ((x >= chunk) & (s >= chunk) & (v <= u) & ok_up))

    def collect(m):
        for d in range(1, MID):
            give(m, d, receive=True).wait_recv()
            forward(m, d)

    def classes(x):
        x4 = x.reshape(MID, NS, mm, e)
        return [x4[:, n].reshape(chunk, e) for n in range(NS)]

    def unclass(parts):
        return jnp.concatenate([parts[n][i * mm:(i + 1) * mm] for i in range(MID) for n in range(NS)], axis=0)

    def with_ones(x):
        return jnp.concatenate([x, jnp.ones((x.shape[0], e), BF16)], axis=1)

    def prob(s, top):
        return jnp.exp2((s - top) * SCALE).astype(BF16)

    def home_plane(m):
        q = qp[m].reshape(rows, e)
        kh, vh = kv[1, m, 0].reshape(rows, e), kv[1, m, 1].reshape(rows, e)
        mid = [nt(q[i * half:(i + 1) * half], kh[i * chunk:(i + 3) * chunk]) + mid_bias[i] for i in range(2)]
        mid = jnp.concatenate(mid, axis=0)
        far = unclass([nt(a, b) for a, b in zip(classes(q), classes(kh))])
        top = jnp.maximum(
            jnp.max(mid[:, :2 * chunk], axis=-1, keepdims=True),
            jnp.max(jnp.maximum(mid[:, 2 * chunk:], far), axis=-1, keepdims=True))
        p_mid, p_far = prob(mid, top), prob(far, top)
        total = jnp.concatenate([
            nn(p_mid[i * half:(i + 1) * half], with_ones(vh[i * chunk:(i + 3) * chunk])) for i in range(2)], axis=0)
        p4 = p_far.reshape(MID, NS, mm, chunk)
        total += unclass([nn(p4[:, n].reshape(chunk, chunk), with_ones(v)) for n, v in enumerate(classes(vh))])
        o_s[m] = total[:, :e].reshape(MID, chunk, e)
        d_s[m] = total[:, e:].reshape(MID, chunk, e)
        t_s[m] = jnp.broadcast_to(top, (rows, e)).reshape(MID, chunk, e)

    def find_ends():
        x, s = iota((2 * SIDE, rows), 0), iota((2 * SIDE, rows), 1)
        pick = (token(s) == x + (x // SIDE) * (rows - 2 * SIDE)).astype(BF16)
        for b in range(MID):
            both = jnp.concatenate([kv[1, :, 0, b].reshape(rows, e), kv[1, :, 1, b].reshape(rows, e)], axis=1)
            both = nn(pick, both).astype(BF16)
            for side in range(2):
                for n in range(2):
                    ends[side, b, n] = both[side * SIDE:(side + 1) * SIDE, n * e:(n + 1) * e]

    lane = iota((1, 2 * SIDE), 1)

    def near(b):
        q = qp[:, b].reshape(rows, e)
        kb, vb = kv[1, :, 0, b].reshape(rows, e), kv[1, :, 1, b].reshape(rows, e)
        lo = [ends[1, b - 1, n] if b > 0 else edge_out[0, n] for n in range(2)]
        hi = [ends[0, b + 1, n] if b < last else edge_out[1, n] for n in range(2)]
        k_rim, v_rim = (jnp.concatenate([lo[n], hi[n]], axis=0) for n in range(2))
        own = nt(q, kb) + near_bias[:, :rows]
        rim = nt(q, k_rim) + near_bias[:, rows:]
        if b == 0:
            rim += bias((lane >= SIDE) | ok_dn)
        if b == last:
            rim += bias((lane < SIDE) | ok_up)
        old = t_s[:, b].reshape(rows, e)
        peak = jnp.maximum(jnp.maximum(own[:, :e], own[:, e:]), rim)
        top = jnp.maximum(old, jnp.max(peak, axis=-1, keepdims=True))
        fade = jnp.exp2((old - top) * SCALE)
        both = jnp.concatenate([top, top], axis=1)
        total = nn(prob(own, both), with_ones(vb)) + nn(prob(rim, top), with_ones(v_rim))
        o_s[:, b] = (fade * o_s[:, b].reshape(rows, e) + total[:, :e]).reshape(MID, chunk, e)
        d_s[:, b] = (fade * d_s[:, b].reshape(rows, e) + total[:, e:]).reshape(MID, chunk, e)
        t_s[:, b] = top.reshape(MID, chunk, e)

    def other_planes(m):
        q = qp[m].reshape(rows, e)
        k2 = [[kv[i, m, n].reshape(rows, e) for n in range(2)] for i in (0, 2)]
        cat = lambda a, b: jnp.concatenate([a, b], axis=0)
        k_far = [cat(a, b) for a, b in zip(classes(k2[0][0]), classes(k2[1][0]))]
        v_far = [cat(a, b) for a, b in zip(classes(k2[0][1]), classes(k2[1][1]))]
        far = unclass([nt(a, b) + far_bias[...] for a, b in zip(classes(q), k_far)])
        k_rim, v_rim = (cat(k2[0][n][last * chunk:], k2[1][n][:chunk]) for n in range(2))
        rim = nt(cat(q[:chunk], q[last * chunk:]), k_rim) + rim_bias[...]
        peak = jnp.concatenate([
            jnp.maximum(far[:chunk], rim[:chunk]), far[chunk:last * chunk],
            jnp.maximum(far[last * chunk:], rim[chunk:])], axis=0)
        old = t_s[m].reshape(rows, e)
        top = jnp.maximum(old, jnp.max(peak, axis=-1, keepdims=True))
        fade = jnp.exp2((old - top) * SCALE)
        p4 = prob(far, top).reshape(MID, NS, mm, 2 * chunk)
        total = unclass([nn(p4[:, n].reshape(chunk, 2 * chunk), with_ones(v)) for n, v in enumerate(v_far)])
        extra = nn(prob(rim, cat(top[:chunk], top[last * chunk:])), with_ones(v_rim))
        total = jnp.concatenate([
            total[:chunk] + extra[:chunk], total[chunk:last * chunk], total[last * chunk:] + extra[chunk:]], axis=0)
        o = fade * o_s[m].reshape(rows, e) + total[:, :e]
        den = fade * d_s[m].reshape(rows, e) + total[:, e:]
        ob[m] = (o / den).astype(BF16).reshape(MID, chunk, e)

    def cols(core, head):
        return pl.ds(pl.multiple_of(core * width + head * e, e), e)

    def result(m, d, receive=False):
        head = (j - d + MID) % MID if receive else j
        return remote(ob.at[m, (j + d) % MID], att.at[m, :, cols(c, head)],
                      res_s.at[m, d - 1], res_r.at[m, d - 1], mate(d), c)

    def across(d, receive=False):
        core, head = (1 - c, (j - d + MID) % MID) if receive else (c, j)
        return remote(ob.at[last, (j + d) % MID], att.at[last, :, cols(core, head)],
                      cross_s.at[d], cross_r.at[d], mate(d), 1 - c)

    def share(m):
        side = pl.ds(pl.multiple_of(c * width, width), width)
        return remote(att.at[m, :, side], att.at[m, :, side], tp_s.at[m], tp_r.at[m], p, 1 - c)

    def share_in(m):
        side = pl.ds(pl.multiple_of((1 - c) * width, width), width)
        return remote(att.at[m, :, side], att.at[m, :, side], tp_s.at[m], tp_r.at[m], p, 1 - c)

    def finish(m):
        @pl.when(has_dn)
        def _():
            for d in range(MID):
                up(m, d).wait_recv()

        @pl.when(has_up)
        def _():
            for d in range(MID):
                down(m, d).wait_recv()

        other_planes(m)
        for d in range(1, MID):
            result(m, d).start()
        if m == last:
            for d in range(MID):
                across(d).start()
        att[m, :, cols(c, j)] = ob[m, pl.ds(j, 1)].reshape(chunk, e)

    collect(0)
    collect(1)
    for side in range(2):
        @pl.when(has[side] & jnp.logical_not(homes[side]))
        def _():
            for n in range(2):
                rim_in(side, n, 1).wait_recv()
                rim_out(side, n, False).start()
    for d in range(1, MID):
        ask(0, d, receive=True).wait_recv()
    home_plane(0)
    collect(2)
    home_plane(1)
    collect(3)
    for d in range(1, MID):
        ask(1, d, receive=True).wait_recv()
    home_plane(2)
    home_plane(3)
    find_ends()
    for side in range(2):
        @pl.when(has[1 - side])
        def _():
            for n in range(2):
                rim_out(side, n, False).wait_recv()
    for b in range(MID):
        near(b)
    for m in range(MID):
        finish(m)

    for m in range(last):
        for d in range(1, MID):
            result(m, d, receive=True).wait_recv()
        share(m).start()
    loads[3].wait()
    for m in range(last):
        share_in(m).wait_recv()
    ys[:last * chunk] = nn(att[:last].reshape(last * chunk, 2 * width), w_in[...]).astype(BF16)
    for d in range(1, MID):
        result(last, d, receive=True).wait_recv()
    for d in range(MID):
        across(d, receive=True).wait_recv()
    ys[last * chunk:] = nn(att[last], w_in[...]).astype(BF16)
    out_ref[...] = nn(back, ys[...]).astype(BF16)

    for m in range(MID):
        for d in range(1, MID):
            give(m, d).wait_send()
            result(m, d).wait_send()
    for d in range(MID):
        across(d).wait_send()
    for m in range(last):
        share(m).wait_send()
    for i in range(2):
        for d in range(1, MID):
            ask(i, d).wait_send()

    @pl.when(has_up)
    def _():
        for m in range(MID):
            for d in range(MID):
                up(m, d).wait_send()

    @pl.when(has_dn)
    def _():
        for m in range(MID):
            for d in range(MID):
                down(m, d).wait_send()

    for side in range(2):
        @pl.when(has[side])
        def _():
            for n in range(2):
                rim_out(side, n, False).wait_send()

        @pl.when(has[side] & homes[side])
        def _():
            for n in range(2):
                for d in range(1, MID):
                    rim_in(side, n, d).wait_send()


def per_device(sp_n, q, k, v, w):
    rows, columns = q.shape
    heads = columns // HEAD_DIM
    assert MID * rows == SIDE * FAR and rows // MID == SIDE and sp_n % MID == 0 and heads == MID
    dma = pltpu.SemaphoreType.DMA
    e, chunk = HEAD_DIM, rows // MID
    vmem = lambda *shape, dtype=BF16: pltpu.VMEM(shape, dtype)
    pinned = [pltpu.with_memory_space_constraint(x, pltpu.HBM) for x in (q, k, v, w)]
    return pl.pallas_call(
        functools.partial(kernel, sp_n, heads),
        out_shape=pltpu.VMEM((rows, w.shape[1]), BF16),
        in_specs=[pl.BlockSpec(memory_space=pltpu.HBM)] * 4,
        out_specs=pl.BlockSpec(memory_space=pltpu.VMEM),
        scratch_shapes=[
            vmem(rows, columns), vmem(rows, columns), vmem(rows, columns), vmem(*w.shape),
            vmem(MID, heads, 3, chunk, e),
            vmem(3, MID, 2, MID, chunk, e),
            vmem(MID, MID, chunk, e),
            vmem(2, 2, SIDE, e), vmem(2, 2, SIDE, e),
            vmem(2, MID, 2, SIDE, e),
            vmem(rows, rows + 2 * SIDE, dtype=F32),
            vmem(2, rows // 2, 3 * chunk, dtype=F32),
            vmem(chunk, 2 * chunk, dtype=F32),
            vmem(rows // 2, 2 * chunk, dtype=F32),
            vmem(MID, MID, chunk, e, dtype=F32), vmem(MID, MID, chunk, e, dtype=F32), vmem(MID, MID, chunk, e, dtype=F32),
            vmem(MID, MID, chunk, e),
            vmem(MID, chunk, 2 * columns),
            vmem(rows, w.shape[1]),
            dma((4,)),
            dma((MID, MID - 1)), dma((MID, MID - 1)),
            dma((2, MID - 1)), dma((2, MID - 1)),
            dma((MID, MID)), dma((MID, MID)),
            dma((MID, MID)), dma((MID, MID)),
            dma((2, 2, MID - 1)), dma((2, 2)),
            dma((2, 2)), dma((2, 2)),
            dma((MID, MID - 1)), dma((MID, MID - 1)),
            dma((MID,)), dma((MID,)),
            dma((MID,)), dma((MID,)),
        ],
        compiler_params=pltpu.CompilerParams(
            collective_id=0, has_side_effects=True, vmem_limit_bytes=40 * 1024 * 1024),
    )(*pinned)


def solution(mesh):
    return jax.shard_map(
        functools.partial(per_device, mesh.shape["sp"]), mesh=mesh,
        in_specs=(P("sp", "tp"), P("sp", "tp"), P("sp", "tp"), P(None, "tp")),
        out_specs=P("sp", "tp"), check_vma=False,
    )
```

time: 28.2 us -> 27.3 us (0.968)
  matrix products: 1.51 us -> 0 us
  local copies, waits for them, and re-layouts: 0.01 us -> 0.8 us
    dot_general x1 -> x0, matrix products: 1.51 us -> none  [nn(): lax.dot_general(a, b, (((1,), (0,)), ((), ())), preferred_element_type=F32)]
    unnamed x2 -> x1, local copies, waits for them, and re-layouts: 0.01 us -> 0.8 us
where the time goes in v2:
time: 27.3 us; the launch traced here: 27.1 us
  Pallas kernels  26.2 us (96%)
  local copies, waits for them, and re-layouts  0.8 us (3%)
    pallas_call x1, Pallas kernels, per_device(): pl.pallas_call(functools.partial(kernel, sp_n, heads), out_shape=pltpu.VM...  26.2 us
    unnamed x1, local copies, waits for them, and re-layouts  0.8 us

profile of v2, /device:TPU:1, one launch (start us, length us, event | category | flops | bytes accessed | tf_op | source)
XLA Modules:
  0.0 27.1 jit_solution(12625460795858981956)
XLA Ops:
  0.0 26.2 %shard_map.46 = bf16[256,1024]{1,0:T(8,128)(2,1)S(1)} custom-call(bf16[256,512]{1,0:T(8,128)(2,1)} %q_hbm.1, bf16[256,512]{1,0:T(8,128)(2,1)} %k_hbm.1, bf16[256,512]{1,0:T(8,128)(2,1)} %v_hbm.1, bf16[1024,1024]{1,0:T(8,128)(2,1)} %w_hbm.1), custom_call_target="tpu_custom_call" | custom-call | tf_op jit(solution)/shard_map/pallas_call | solution.py:431
  26.3 0.8 %copy.6 = bf16[256,1024]{1,0:T(8,128)(2,1)} copy(bf16[256,1024]{1,0:T(8,128)(2,1)S(1)} %shard_map.46) | data formatting | bytes 1048576

commit v3 on v2

v3 whole, which is shorter than its diff:
```python
import functools
import math

import jax
import jax.numpy as jnp
from jax import lax
from jax.experimental import pallas as pl
from jax.experimental.pallas import tpu as pltpu
from jax.sharding import PartitionSpec as P

HEAD_DIM = 128
SIDE = 64
MID = 4
FAR = 16
NS = FAR // MID
MESH = pl.DeviceIdType.MESH
F32 = jnp.float32
BF16 = jnp.bfloat16
SCALE = HEAD_DIM ** -0.5 * math.log2(math.e)
NEG = -jnp.inf
EARLY = 2


def nt(a, b):
    return lax.dot_general(a, b, (((1,), (1,)), ((), ())), preferred_element_type=F32)


def nn(a, b):
    return lax.dot_general(a, b, (((1,), (0,)), ((), ())), preferred_element_type=F32)


def iota(shape, dim):
    return lax.broadcasted_iota(jnp.int32, shape, dim)


def bias(ok):
    return jnp.where(ok, 0.0, NEG).astype(F32)


def kernel(sp_n, heads, q_hbm, k_hbm, v_hbm, w_hbm, out_ref,
           q_in, k_in, v_in, w_in, ps, kv, qp, ends, outer, near_bias, mid_bias, far_bias, rim_bias,
           o_s, t_s, d_s, ob, att, natural,
           load_sem, give_s, give_r, ask_s, ask_r, up_s, up_r, dn_s, dn_r, res_s, res_r, cross_s, cross_r, tp_s, tp_r):
    rows = q_in.shape[0]
    chunk = rows // MID
    mm = rows // FAR
    e = HEAD_DIM
    width = heads * e
    last = MID - 1
    p, c = lax.axis_index("sp"), lax.axis_index("tp")
    groups = sp_n // MID
    g, j = p // MID, p % MID

    loads = [
        pltpu.make_async_copy(src, dst, load_sem.at[n])
        for n, (src, dst) in enumerate(((k_hbm, k_in), (v_hbm, v_in), (q_hbm, q_in), (w_hbm, w_in)))
    ]
    for load in loads[:3]:
        load.start()

    barrier = pltpu.get_barrier_semaphore()

    def greet(sp, tp):
        pl.semaphore_signal(barrier, inc=1, device_id=(sp, tp), device_id_type=MESH)

    others = (MID - 1 - j, j + 1 - 2 * (j % 2), (j + MID // 2) % MID)

    def mate(d):
        return g * MID + others[d]

    for d in range(last):
        greet(mate(d), c)
        greet(mate(d), 1 - c)
    greet(p, 1 - c)
    has_dn, has_up = g > 0, g < groups - 1
    up_p, dn_p = (p + MID) % sp_n, (p - MID + sp_n) % sp_n

    @pl.when(has_dn)
    def _():
        greet(dn_p, c)

    @pl.when(has_up)
    def _():
        greet(up_p, c)

    def remote(src, dst, ss, rs, sp, tp):
        return pltpu.make_async_remote_copy(
            src_ref=src, dst_ref=dst, send_sem=ss, recv_sem=rs, device_id=(sp, tp), device_id_type=MESH)

    def await_all(ref, sem):
        pltpu.make_async_copy(ref, ref, sem).wait()

    def token(r):
        return FAR * (r % mm) + MID * ((r % chunk) // mm) + r // chunk

    r, t = iota((rows, rows), 0), iota((rows, rows), 1)
    perm = (t == token(r)).astype(BF16)

    def reorder(n, x):
        loads[n].wait()
        moved = nn(perm, x[...]).astype(BF16)
        for h in range(heads):
            for m in range(MID):
                ps[m, h, n] = moved[m * chunk:(m + 1) * chunk, h * e:(h + 1) * e]

    reorder(0, k_in)
    reorder(1, v_in)

    @pl.when(jnp.logical_not(has_dn))
    def _():
        kv[0] = jnp.zeros(kv.shape[1:], BF16)

    @pl.when(jnp.logical_not(has_up))
    def _():
        kv[2] = jnp.zeros(kv.shape[1:], BF16)

    pl.semaphore_wait(barrier, 2 * MID - 1 + has_dn.astype(jnp.int32) + has_up.astype(jnp.int32))

    pair = pl.ds(0, 2)

    def give(m, d):
        return remote(ps.at[m, others[d], pair], kv.at[1, m, :, j], give_s.at[0], give_r.at[m, j], mate(d), c)

    def ask(i, d):
        two = pl.ds(2 * i, 2)
        return remote(ps.at[two, others[d], 2], qp.at[two, j], ask_s.at[0], ask_r.at[i], mate(d), c)

    def up(m, b, own=False):
        src = ps.at[m, j, pair] if own else kv.at[1, m, :, b]
        arrived = (b == last).astype(jnp.int32) * MID + (b != last).astype(jnp.int32) * m if own else (MID if b == last else m)
        return remote(src, kv.at[0, m, :, b], up_s.at[0], up_r.at[arrived], up_p, c)

    def down(m, b, own=False):
        src = ps.at[m, j, pair] if own else kv.at[1, m, :, b]
        arrived = (b == 0).astype(jnp.int32) * MID + (b != 0).astype(jnp.int32) * m if own else (MID if b == 0 else m)
        return remote(src, kv.at[2, m, :, b], dn_s.at[0], dn_r.at[arrived], dn_p, c)

    for m in range(MID):
        for d in range(last):
            give(m, d).start()
        if m == 0:
            @pl.when(has_up)
            def _():
                for i in range(MID):
                    up(i, j, own=True).start()

            @pl.when(has_dn)
            def _():
                for i in range(MID):
                    down(i, j, own=True).start()

    reorder(2, q_in)
    for i in range(2):
        for d in range(last):
            ask(i, d).start()

    loads[3].start()
    for m in range(MID):
        kv[1, m, :, pl.ds(j, 1)] = ps[m, pl.ds(j, 1), 0:2].reshape(2, 1, chunk, e)
        qp[m, pl.ds(j, 1)] = ps[m, pl.ds(j, 1), 2]

    ok_dn, ok_up = has_dn.astype(jnp.int32) == 1, has_up.astype(jnp.int32) == 1
    tq, s = token(iota((rows, rows), 0)), iota((rows, rows), 1)
    gap = tq - token(s)
    near_bias[:, :rows] = bias((gap >= -SIDE) & (gap <= SIDE))
    tq, s = token(iota((rows, 2 * SIDE), 0)), iota((rows, 2 * SIDE), 1)
    near_bias[:, rows:] = bias(((s < SIDE) & (s >= tq)) | ((s >= SIDE) & (s - SIDE <= tq - (rows - SIDE))))

    def order(x):
        return chunk * (x // chunk) + NS * (x % mm) + (x % chunk) // mm

    half = rows // 2
    uq, uk = order(iota((half, 3 * chunk), 0)), order(iota((half, 3 * chunk), 1))
    for i in range(2):
        gap = uk - uq - i * chunk
        mid_bias[i] = bias((gap >= -SIDE) & (gap <= SIDE))
    x, s = iota((chunk, 2 * chunk), 0), iota((chunk, 2 * chunk), 1)
    far_bias[...] = bias(((s < chunk) & (s >= x) & ok_dn) | ((s >= chunk) & (s - chunk <= x) & ok_up))
    x, s = iota((half, 2 * chunk), 0), iota((half, 2 * chunk), 1)
    u, v = order(x % chunk), order(s % chunk)
    low, high = (x < chunk) & (s < chunk) & ok_dn, (x >= chunk) & (s >= chunk) & ok_up
    for m in range(MID):
        tq = token(m * chunk + x % chunk)
        rim_bias[m, :, :2 * chunk] = bias((low & (v >= u)) | (high & (v <= u)))
        rim_bias[m, :, 2 * chunk:] = bias((low & (s >= tq)) | (high & (s - SIDE <= tq - (rows - SIDE))))

    def arrival(m, b, rise, fall):
        @pl.when(j != b)
        def _():
            await_all(kv.at[1, m, :, b], give_r.at[m, b])

        relay(m, b, rise, fall)

    def relay(m, b, rise, fall):
        if rise:
            @pl.when((j != b) & has_up)
            def _():
                up(m, b).start()

        if fall:
            @pl.when((j != b) & has_dn)
            def _():
                down(m, b).start()

    def classes(x):
        x4 = x.reshape(MID, NS, mm, e)
        return [x4[:, n].reshape(chunk, e) for n in range(NS)]

    def unclass(parts):
        return jnp.concatenate([parts[n][i * mm:(i + 1) * mm] for i in range(MID) for n in range(NS)], axis=0)

    def cat(*parts):
        return jnp.concatenate(parts, axis=0)

    def with_ones(x):
        return jnp.concatenate([x, jnp.ones((x.shape[0], e), BF16)], axis=1)

    def prob(s, top):
        return jnp.exp2((s - top) * SCALE).astype(BF16)

    x, s = iota((2 * SIDE, rows), 0), iota((2 * SIDE, rows), 1)
    pick = (token(s) == x + (x // SIDE) * (rows - 2 * SIDE)).astype(BF16)

    def both(i, b):
        return jnp.concatenate([kv[i, :, n, b].reshape(rows, e) for n in range(2)], axis=1)

    def find_ends():
        for b in range(MID):
            x = nn(pick, both(1, b)).astype(BF16)
            for side in range(2):
                for n in range(2):
                    ends[side, b, n] = x[side * SIDE:(side + 1) * SIDE, n * e:(n + 1) * e]

    def find_outer():
        x = cat(nn(pick[SIDE:], both(0, last)), nn(pick[:SIDE], both(2, 0))).astype(BF16)
        for n in range(2):
            outer[n] = x[:, n * e:(n + 1) * e]

    lane = iota((1, 2 * SIDE), 1)

    def middle(m):
        q = qp[m].reshape(rows, e)
        kh, vh = kv[1, m, 0].reshape(rows, e), kv[1, m, 1].reshape(rows, e)
        mid = cat(*[nt(q[i * half:(i + 1) * half], kh[i * chunk:(i + 3) * chunk]) + mid_bias[i] for i in range(2)])
        top = jnp.maximum(jnp.max(mid[:, :e], axis=-1, keepdims=True), jnp.max(mid[:, e:], axis=-1, keepdims=True))
        p_mid = prob(mid, top)
        total = cat(*[nn(p_mid[i * half:(i + 1) * half], with_ones(vh[i * chunk:(i + 3) * chunk])) for i in range(2)])
        o_s[m] = total[:, :e]
        d_s[m] = total[:, e:]
        t_s[m] = jnp.broadcast_to(top, (rows, e))

    def near(b):
        q = qp[:, b].reshape(rows, e)
        kb, vb = kv[1, :, 0, b].reshape(rows, e), kv[1, :, 1, b].reshape(rows, e)
        k_rim, v_rim = (cat(ends[1, max(b - 1, 0), n], ends[0, min(b + 1, last), n]) for n in range(2))
        own = nt(q, kb) + near_bias[:, :rows]
        rim = nt(q, k_rim) + near_bias[:, rows:]
        if b == 0:
            rim += bias(lane >= SIDE)
        if b == last:
            rim += bias(lane < SIDE)
        at_b = pl.ds(b * chunk, chunk)
        old = t_s[:, at_b].reshape(rows, e)
        peak = jnp.maximum(jnp.maximum(own[:, :e], own[:, e:]), rim)
        top = jnp.maximum(old, jnp.max(peak, axis=-1, keepdims=True))
        fade = jnp.exp2((old - top) * SCALE)
        both = jnp.concatenate([top, top], axis=1)
        total = nn(prob(own, both), with_ones(vb)) + nn(prob(rim, top), with_ones(v_rim))
        o_s[:, at_b] = (fade * o_s[:, at_b].reshape(rows, e) + total[:, :e]).reshape(MID, chunk, e)
        d_s[:, at_b] = (fade * d_s[:, at_b].reshape(rows, e) + total[:, e:]).reshape(MID, chunk, e)
        t_s[:, at_b] = top.reshape(MID, chunk, e)

    def other_planes(m):
        q = qp[m].reshape(rows, e)
        k2 = [[kv[i, m, n].reshape(rows, e) for n in range(2)] for i in (0, 2, 1)]
        k_far, v_far = ([cat(*x) for x in zip(*(classes(k2[i][n]) for i in range(3)))] for n in range(2))
        far = [nt(a, b) for a, b in zip(classes(q), k_far)]
        near_far, own = unclass([x[:, :e] + far_bias[...] for x in far]), unclass([x[:, e:] for x in far])
        far = near_far
        k_rim, v_rim = (cat(k2[0][n][last * chunk:], k2[1][n][:chunk], outer[n]) for n in range(2))
        rim = nt(cat(q[:chunk], q[last * chunk:]), k_rim) + rim_bias[m]
        peak = jnp.maximum(rim[:, :e], rim[:, e:])
        peak = cat(jnp.maximum(far[:chunk], peak[:chunk]), far[chunk:last * chunk],
                   jnp.maximum(far[last * chunk:], peak[chunk:]))
        old = t_s[m]
        top = jnp.maximum(old, jnp.maximum(
            jnp.max(peak, axis=-1, keepdims=True), jnp.max(own, axis=-1, keepdims=True)))
        fade = jnp.exp2((old - top) * SCALE)
        p4 = jnp.concatenate([prob(far, top), prob(own, top[:, :chunk])], axis=1).reshape(MID, NS, mm, 3 * chunk)
        total = unclass([nn(p4[:, n].reshape(chunk, 3 * chunk), with_ones(v)) for n, v in enumerate(v_far)])
        top = cat(top[:chunk], top[last * chunk:])
        extra = nn(prob(rim, jnp.concatenate([top, top], axis=1)), with_ones(v_rim))
        total = cat(total[:chunk] + extra[:chunk], total[chunk:last * chunk], total[last * chunk:] + extra[chunk:])
        o = fade * o_s[m] + total[:, :e]
        den = fade * d_s[m] + total[:, e:]
        ob[m] = (o / den).astype(BF16).reshape(MID, chunk, e)

    def cols(core, head):
        return pl.ds(pl.multiple_of(core * width + head * e, e), e)

    def side(core):
        return pl.ds(pl.multiple_of(core * width, width), width)

    def result(m, d):
        return remote(ob.at[m, others[d]], att.at[m, :, cols(c, j)], res_s.at[0], res_r.at[m], mate(d), c)

    def across(m, b, to):
        return remote(ob.at[m, b], att.at[m, :, cols(c, j)], cross_s.at[0], cross_r.at[m - EARLY], to, 1 - c)

    def share(m):
        return remote(att.at[m, :, side(c)], att.at[m, :, side(c)], tp_s.at[0], tp_r.at[max(m - EARLY + 1, 0)], p, 1 - c)

    early = tuple(range(EARLY))
    late = tuple(range(EARLY, MID))

    def finish(ms):
        @pl.when(has_dn)
        def _():
            for m in ms:
                await_all(kv.at[0, m, :, pl.ds(0, last)], up_r.at[m])

        @pl.when(has_up)
        def _():
            for m in ms:
                await_all(kv.at[2, m, :, pl.ds(1, last)], dn_r.at[m])

        for m in ms:
            other_planes(m)
        for m in ms:
            for d in range(last):
                result(m, d).start()
            if m in late:
                @pl.when(c == 0)
                def _():
                    for d in range(last):
                        across(m, others[d], mate(d)).start()
                    across(m, j, p).start()
            att[m, :, cols(c, j)] = ob[m, pl.ds(j, 1)].reshape(chunk, e)

    def project(ms):
        y = nn(att[ms[0]:ms[-1] + 1].reshape(len(ms) * chunk, 2 * width), w_in[...])
        for i, m in enumerate(ms):
            for n in range(NS):
                part = y[i * chunk + n * mm:i * chunk + (n + 1) * mm]
                for t in range(natural.shape[0]):
                    natural[t, pl.ds(MID * n + m, mm, stride=FAR), :] = part[:, t * e:(t + 1) * e]

    for b in range(MID):
        arrival(0, b, True, True)
    for b in range(MID):
        arrival(1, b, True, True)
    for b in range(MID):
        arrival(2, b, b == last, b == 0)
    for b in range(MID):
        arrival(3, b, b == last, b == 0)
    for m in range(2, MID):
        for b in range(MID):
            relay(m, b, b != last, b != 0)
    find_ends()
    await_all(qp.at[pl.ds(0, 2), pl.ds(0, last)], ask_r.at[0])
    middle(0)
    middle(1)
    await_all(qp.at[pl.ds(0, 2), pl.ds(0, last)], ask_r.at[1])
    middle(2)
    middle(3)
    for b in range(MID):
        near(b)
    @pl.when(has_dn)
    def _():
        await_all(kv.at[0, :, :, last], up_r.at[MID])

    @pl.when(has_up)
    def _():
        await_all(kv.at[2, :, :, 0], dn_r.at[MID])

    find_outer()
    finish((0, 1))
    finish((2,))
    finish((3,))
    for m in early:
        await_all(ob.at[m, pl.ds(0, last)], res_r.at[m])
        share(m).start()
    loads[3].wait()
    def project_early():
        await_all(att.at[pl.ds(0, EARLY), :, side(1 - c)], tp_r.at[0])
        project(early)

    @pl.when(c == 0)
    def _():
        project_early()
        for m in late:
            await_all(ob.at[m, pl.ds(0, last)], res_r.at[m])
            await_all(att.at[m, :, side(1 - c)], tp_r.at[m - EARLY + 1])
            project((m,))

    @pl.when(c == 1)
    def _():
        for m in late:
            await_all(ob.at[m, pl.ds(0, last)], res_r.at[m])
            share(m).start()
        for m in late:
            await_all(ob.at[m], cross_r.at[m - EARLY])
            project((m,))
        project_early()

    for t in range(natural.shape[0]):
        out_ref[:, t * e:(t + 1) * e] = natural[t].astype(BF16)

    await_all(ps.at[:, pl.ds(0, last), pair], give_s.at[0])
    await_all(ps.at[:, pl.ds(0, last), 2], ask_s.at[0])
    await_all(ob.at[:, pl.ds(0, last)], res_s.at[0])

    @pl.when(c == 0)
    def _():
        await_all(ob.at[pl.ds(0, MID - EARLY)], cross_s.at[0])
        await_all(att.at[pl.ds(0, EARLY), :, side(c)], tp_s.at[0])

    @pl.when(c == 1)
    def _():
        await_all(att.at[:, :, side(c)], tp_s.at[0])

    @pl.when(has_up)
    def _():
        await_all(kv.at[0], up_s.at[0])

    @pl.when(has_dn)
    def _():
        await_all(kv.at[2], dn_s.at[0])


def per_device(sp_n, q, k, v, w):
    rows, columns = q.shape
    heads = columns // HEAD_DIM
    assert MID * rows == SIDE * FAR and rows // MID == SIDE and sp_n % MID == 0 and heads == MID
    dma = pltpu.SemaphoreType.DMA
    e, chunk = HEAD_DIM, rows // MID
    vmem = lambda *shape, dtype=BF16: pltpu.VMEM(shape, dtype)
    pinned = [pltpu.with_memory_space_constraint(x, pltpu.HBM) for x in (q, k, v, w)]
    return pl.pallas_call(
        functools.partial(kernel, sp_n, heads),
        out_shape=pltpu.VMEM((rows, w.shape[1]), BF16),
        in_specs=[pl.BlockSpec(memory_space=pltpu.HBM)] * 4,
        out_specs=pl.BlockSpec(memory_space=pltpu.VMEM),
        scratch_shapes=[
            vmem(rows, columns), vmem(rows, columns), vmem(rows, columns), vmem(*w.shape),
            vmem(MID, heads, 3, chunk, e),
            vmem(3, MID, 2, MID, chunk, e),
            vmem(MID, MID, chunk, e),
            vmem(2, MID, 2, SIDE, e),
            vmem(2, 2 * SIDE, e),
            vmem(rows, rows + 2 * SIDE, dtype=F32),
            vmem(2, rows // 2, 3 * chunk, dtype=F32),
            vmem(chunk, 2 * chunk, dtype=F32),
            vmem(MID, rows // 2, 4 * chunk, dtype=F32),
            vmem(MID, rows, e, dtype=F32), vmem(MID, rows, e, dtype=F32), vmem(MID, rows, e, dtype=F32),
            vmem(MID, MID, chunk, e),
            vmem(MID, chunk, 2 * columns),
            vmem(w.shape[1] // e, rows, e, dtype=F32),
            dma((4,)),
            dma((1,)), dma((MID, MID)),
            dma((1,)), dma((2,)),
            dma((1,)), dma((MID + 1,)),
            dma((1,)), dma((MID + 1,)),
            dma((1,)), dma((MID,)),
            dma((1,)), dma((MID - EARLY,)),
            dma((1,)), dma((MID - EARLY + 1,)),
        ],
        compiler_params=pltpu.CompilerParams(
            collective_id=0, has_side_effects=True, vmem_limit_bytes=40 * 1024 * 1024),
    )(*pinned)


def solution(mesh):
    return jax.shard_map(
        functools.partial(per_device, mesh.shape["sp"]), mesh=mesh,
        in_specs=(P("sp", "tp"), P("sp", "tp"), P("sp", "tp"), P(None, "tp")),
        out_specs=P("sp", "tp"), check_vma=False,
    )
```

time: 27.3 us -> 24.4 us (0.89)
  Pallas kernels: 26.2 us -> 23.5 us
    pallas_call x1, Pallas kernels: 26.2 us -> 23.5 us  [per_device(): pl.pallas_call(functools.partial(kernel, sp_n, heads), out_shape=pltpu.VM...]
where the time goes in v3:
time: 24.4 us; the launch traced here: 24.3 us
  Pallas kernels  23.5 us (96%)
  local copies, waits for them, and re-layouts  0.8 us (3%)
    pallas_call x1, Pallas kernels, per_device(): pl.pallas_call(functools.partial(kernel, sp_n, heads), out_shape=pltpu.VM...  23.5 us
    unnamed x1, local copies, waits for them, and re-layouts  0.8 us

profile of v3, /device:TPU:1, one launch (start us, length us, event | category | flops | bytes accessed | tf_op | source)
XLA Modules:
  0.0 24.3 jit_solution(192034456390833474)
XLA Ops:
  0.0 23.5 %shard_map.46 = bf16[256,1024]{1,0:T(8,128)(2,1)S(1)} custom-call(bf16[256,512]{1,0:T(8,128)(2,1)} %q_hbm.1, bf16[256,512]{1,0:T(8,128)(2,1)} %k_hbm.1, bf16[256,512]{1,0:T(8,128)(2,1)} %v_hbm.1, bf16[1024,1024]{1,0:T(8,128)(2,1)} %w_hbm.1), custom_call_target="tpu_custom_call" | custom-call | tf_op jit(solution)/shard_map/pallas_call | solution.py:439
  23.5 0.8 %copy.6 = bf16[256,1024]{1,0:T(8,128)(2,1)} copy(bf16[256,1024]{1,0:T(8,128)(2,1)S(1)} %shard_map.46) | data formatting | bytes 1048576

commit v4 on v3

--- a/solution.py
+++ b/solution.py
@@ -39,7 +39,7 @@
 
 def kernel(sp_n, heads, q_hbm, k_hbm, v_hbm, w_hbm, out_ref,
            q_in, k_in, v_in, w_in, ps, kv, qp, ends, outer, near_bias, mid_bias, far_bias, rim_bias,
-           o_s, t_s, d_s, ob, att, natural,
+           o_s, t_s, d_s, ob, att, partial, natural,
            load_sem, give_s, give_r, ask_s, ask_r, up_s, up_r, dn_s, dn_r, res_s, res_r, cross_s, cross_r, tp_s, tp_r):
     rows = q_in.shape[0]
     chunk = rows // MID
@@ -96,15 +96,16 @@
     r, t = iota((rows, rows), 0), iota((rows, rows), 1)
     perm = (t == token(r)).astype(BF16)
 
-    def reorder(n, x):
-        loads[n].wait()
-        moved = nn(perm, x[...]).astype(BF16)
-        for h in range(heads):
-            for m in range(MID):
-                ps[m, h, n] = moved[m * chunk:(m + 1) * chunk, h * e:(h + 1) * e]
-
-    reorder(0, k_in)
-    reorder(1, v_in)
+    def reorder(*arrays):
+        for n, _ in arrays:
+            loads[n].wait()
+        for n, x in arrays:
+            moved = nn(perm, x[...]).astype(BF16)
+            for h in range(heads):
+                for m in range(MID):
+                    ps[m, h, n] = moved[m * chunk:(m + 1) * chunk, h * e:(h + 1) * e]
+
+    reorder((0, k_in), (1, v_in))
 
     @pl.when(jnp.logical_not(has_dn))
     def _():
@@ -119,7 +120,7 @@
     pair = pl.ds(0, 2)
 
     def give(m, d):
-        return remote(ps.at[m, others[d], pair], kv.at[1, m, :, j], give_s.at[0], give_r.at[m, j], mate(d), c)
+        return remote(ps.at[m, others[d], pair], kv.at[1, m, :, j], give_s.at[0], give_r.at[j if m == 0 else last + m], mate(d), c)
 
     def ask(i, d):
         two = pl.ds(2 * i, 2)
@@ -127,16 +128,18 @@
 
     def up(m, b, own=False):
         src = ps.at[m, j, pair] if own else kv.at[1, m, :, b]
-        arrived = (b == last).astype(jnp.int32) * MID + (b != last).astype(jnp.int32) * m if own else (MID if b == last else m)
+        edge = (b == last).astype(jnp.int32) if hasattr(b, "astype") else int(b == last)
+        arrived = edge * MID + (1 - edge) * m
         return remote(src, kv.at[0, m, :, b], up_s.at[0], up_r.at[arrived], up_p, c)
 
     def down(m, b, own=False):
         src = ps.at[m, j, pair] if own else kv.at[1, m, :, b]
-        arrived = (b == 0).astype(jnp.int32) * MID + (b != 0).astype(jnp.int32) * m if own else (MID if b == 0 else m)
+        edge = (b == 0).astype(jnp.int32) if hasattr(b, "astype") else int(b == 0)
+        arrived = edge * MID + (1 - edge) * m
         return remote(src, kv.at[2, m, :, b], dn_s.at[0], dn_r.at[arrived], dn_p, c)
 
     for m in range(MID):
-        for d in range(last):
+        for d in ((1, 2, 0) if m == 0 else range(last)):
             give(m, d).start()
         if m == 0:
             @pl.when(has_up)
@@ -149,7 +152,7 @@
                 for i in range(MID):
                     down(i, j, own=True).start()
 
-    reorder(2, q_in)
+    reorder((2, q_in))
     for i in range(2):
         for d in range(last):
             ask(i, d).start()
@@ -183,13 +186,6 @@
         tq = token(m * chunk + x % chunk)
         rim_bias[m, :, :2 * chunk] = bias((low & (v >= u)) | (high & (v <= u)))
         rim_bias[m, :, 2 * chunk:] = bias((low & (s >= tq)) | (high & (s - SIDE <= tq - (rows - SIDE))))
-
-    def arrival(m, b, rise, fall):
-        @pl.when(j != b)
-        def _():
-            await_all(kv.at[1, m, :, b], give_r.at[m, b])
-
-        relay(m, b, rise, fall)
 
     def relay(m, b, rise, fall):
         if rise:
@@ -337,22 +333,45 @@
                     across(m, j, p).start()
             att[m, :, cols(c, j)] = ob[m, pl.ds(j, 1)].reshape(chunk, e)
 
-    def project(ms):
-        y = nn(att[ms[0]:ms[-1] + 1].reshape(len(ms) * chunk, 2 * width), w_in[...])
+    def half_of(ms, core):
+        x = att[ms[0]:ms[-1] + 1, :, side(core)].reshape(len(ms) * chunk, width)
+        return nn(x, w_in[side(core), :])
+
+    def begin(ms, core):
+        partial[ms[0] * chunk:(ms[-1] + 1) * chunk] = half_of(ms, core)
+
+    def complete(ms, y):
         for i, m in enumerate(ms):
             for n in range(NS):
                 part = y[i * chunk + n * mm:i * chunk + (n + 1) * mm]
                 for t in range(natural.shape[0]):
                     natural[t, pl.ds(MID * n + m, mm, stride=FAR), :] = part[:, t * e:(t + 1) * e]
 
+    def end(ms, core):
+        complete(ms, partial[ms[0] * chunk:(ms[-1] + 1) * chunk] + half_of(ms, core))
+
+    for d in (1, 2, 0):
+        b = others[d]
+        await_all(kv.at[1, 0, :, b], give_r.at[b])
+
+        @pl.when(has_up)
+        def _():
+            up(0, b).start()
+
+        @pl.when(has_dn)
+        def _():
+            down(0, b).start()
+
+    def arrival(m):
+        await_all(kv.at[1, m, :, pl.ds(0, last)], give_r.at[last + m])
+
+    arrival(1)
     for b in range(MID):
-        arrival(0, b, True, True)
-    for b in range(MID):
-        arrival(1, b, True, True)
-    for b in range(MID):
-        arrival(2, b, b == last, b == 0)
-    for b in range(MID):
-        arrival(3, b, b == last, b == 0)
+        relay(1, b, True, True)
+    for m in range(2, MID):
+        arrival(m)
+        relay(m, last, True, False)
+        relay(m, 0, False, True)
     for m in range(2, MID):
         for b in range(MID):
             relay(m, b, b != last, b != 0)
@@ -381,27 +400,31 @@
         await_all(ob.at[m, pl.ds(0, last)], res_r.at[m])
         share(m).start()
     loads[3].wait()
-    def project_early():
-        await_all(att.at[pl.ds(0, EARLY), :, side(1 - c)], tp_r.at[0])
-        project(early)
-
     @pl.when(c == 0)
     def _():
-        project_early()
+        begin(early, 0)
+        await_all(att.at[pl.ds(0, EARLY), :, side(1)], tp_r.at[0])
+        end(early, 1)
+        for m in late:
+            await_all(att.at[m, :, side(1)], tp_r.at[m - EARLY + 1])
+        begin(late, 1)
         for m in late:
             await_all(ob.at[m, pl.ds(0, last)], res_r.at[m])
-            await_all(att.at[m, :, side(1 - c)], tp_r.at[m - EARLY + 1])
-            project((m,))
+            end((m,), 0)
 
     @pl.when(c == 1)
     def _():
         for m in late:
             await_all(ob.at[m, pl.ds(0, last)], res_r.at[m])
             share(m).start()
-        for m in late:
+        begin(tuple(range(MID)), 1)
+        await_all(ob.at[late[0]], cross_r.at[0])
+        end(late[:1], 0)
+        await_all(att.at[pl.ds(0, EARLY), :, side(0)], tp_r.at[0])
+        end(early, 0)
+        for m in late[1:]:
             await_all(ob.at[m], cross_r.at[m - EARLY])
-            project((m,))
-        project_early()
+            end((m,), 0)
 
     for t in range(natural.shape[0]):
         out_ref[:, t * e:(t + 1) * e] = natural[t].astype(BF16)
@@ -455,9 +478,10 @@
             vmem(MID, rows, e, dtype=F32), vmem(MID, rows, e, dtype=F32), vmem(MID, rows, e, dtype=F32),
             vmem(MID, MID, chunk, e),
             vmem(MID, chunk, 2 * columns),
+            vmem(rows, w.shape[1], dtype=F32),
             vmem(w.shape[1] // e, rows, e, dtype=F32),
             dma((4,)),
-            dma((1,)), dma((MID, MID)),
+            dma((1,)), dma((2 * MID - 1,)),
             dma((1,)), dma((2,)),
             dma((1,)), dma((MID + 1,)),
             dma((1,)), dma((MID + 1,)),

time: 24.4 us -> 24.1 us (0.988); the launches traced: 24.3 us -> 23.7 us
  Pallas kernels: 23.5 us -> 22.9 us
    pallas_call x1, Pallas kernels: 23.5 us -> 22.9 us  [per_device(): pl.pallas_call(functools.partial(kernel, sp_n, heads), out_shape=pltpu.VM...]
where the time goes in v4:
time: 24.1 us; the launch traced here: 23.7 us
  Pallas kernels  22.9 us (95%)
  local copies, waits for them, and re-layouts  0.8 us (3%)
    pallas_call x1, Pallas kernels, per_device(): pl.pallas_call(functools.partial(kernel, sp_n, heads), out_shape=pltpu.VM...  22.9 us
    unnamed x1, local copies, waits for them, and re-layouts  0.8 us

profile of v4, /device:TPU:1, one launch (start us, length us, event | category | flops | bytes accessed | tf_op | source)
XLA Modules:
  0.0 23.7 jit_solution(15638411532526686431)
XLA Ops:
  0.0 22.9 %shard_map.46 = bf16[256,1024]{1,0:T(8,128)(2,1)S(1)} custom-call(bf16[256,512]{1,0:T(8,128)(2,1)} %q_hbm.1, bf16[256,512]{1,0:T(8,128)(2,1)} %k_hbm.1, bf16[256,512]{1,0:T(8,128)(2,1)} %v_hbm.1, bf16[1024,1024]{1,0:T(8,128)(2,1)} %w_hbm.1), custom_call_target="tpu_custom_call" | custom-call | tf_op jit(solution)/shard_map/pallas_call | solution.py:462
  22.9 0.8 %copy.6 = bf16[256,1024]{1,0:T(8,128)(2,1)} copy(bf16[256,1024]{1,0:T(8,128)(2,1)S(1)} %shard_map.46) | data formatting | bytes 1048576

commit v5 on v4

--- a/solution.py
+++ b/solution.py
@@ -245,16 +245,22 @@
         d_s[m] = total[:, e:]
         t_s[m] = jnp.broadcast_to(top, (rows, e))
 
-    def near(b):
+    def rims(b, n):
+        return cat(ends[1, max(b - 1, 0), n], ends[0, min(b + 1, last), n])
+
+    def near_scores(b):
         q = qp[:, b].reshape(rows, e)
-        kb, vb = kv[1, :, 0, b].reshape(rows, e), kv[1, :, 1, b].reshape(rows, e)
-        k_rim, v_rim = (cat(ends[1, max(b - 1, 0), n], ends[0, min(b + 1, last), n]) for n in range(2))
-        own = nt(q, kb) + near_bias[:, :rows]
+        k_rim = rims(b, 0)
+        own = nt(q, kv[1, :, 0, b].reshape(rows, e)) + near_bias[:, :rows]
         rim = nt(q, k_rim) + near_bias[:, rows:]
         if b == 0:
             rim += bias(lane >= SIDE)
         if b == last:
             rim += bias(lane < SIDE)
+        return own, rim
+
+    def near(b, own, rim):
+        vb, v_rim = kv[1, :, 1, b].reshape(rows, e), rims(b, 1)
         at_b = pl.ds(b * chunk, chunk)
         old = t_s[:, at_b].reshape(rows, e)
         peak = jnp.maximum(jnp.maximum(own[:, :e], own[:, e:]), rim)
@@ -320,6 +326,8 @@
             for m in ms:
                 await_all(kv.at[2, m, :, pl.ds(1, last)], dn_r.at[m])
 
+        if ms[0] == 0:
+            find_outer()
         for m in ms:
             other_planes(m)
         for m in ms:
@@ -381,9 +389,11 @@
     middle(1)
     await_all(qp.at[pl.ds(0, 2), pl.ds(0, last)], ask_r.at[1])
     middle(2)
+    scores = near_scores(0)
     middle(3)
     for b in range(MID):
-        near(b)
+        now, scores = scores, near_scores(b + 1) if b < last else None
+        near(b, *now)
     @pl.when(has_dn)
     def _():
         await_all(kv.at[0, :, :, last], up_r.at[MID])
@@ -392,7 +402,6 @@
     def _():
         await_all(kv.at[2, :, :, 0], dn_r.at[MID])
 
-    find_outer()
     finish((0, 1))
     finish((2,))
     finish((3,))

time: 24.1 us -> 23.9 us (level)
  no operation moved by 1% of the time
where the time goes in v5:
time: 23.9 us; the launch traced here: 23.5 us
  Pallas kernels  22.7 us (95%)
  local copies, waits for them, and re-layouts  0.8 us (3%)
    pallas_call x1, Pallas kernels, per_device(): pl.pallas_call(functools.partial(kernel, sp_n, heads), out_shape=pltpu.VM...  22.7 us
    unnamed x1, local copies, waits for them, and re-layouts  0.8 us

profile of v5, /device:TPU:1, one launch (start us, length us, event | category | flops | bytes accessed | tf_op | source)
XLA Modules:
  0.0 23.5 jit_solution(8795382594388774138)
XLA Ops:
  0.0 22.7 %shard_map.46 = bf16[256,1024]{1,0:T(8,128)(2,1)S(1)} custom-call(bf16[256,512]{1,0:T(8,128)(2,1)} %q_hbm.1, bf16[256,512]{1,0:T(8,128)(2,1)} %k_hbm.1, bf16[256,512]{1,0:T(8,128)(2,1)} %v_hbm.1, bf16[1024,1024]{1,0:T(8,128)(2,1)} %w_hbm.1), custom_call_target="tpu_custom_call" | custom-call | tf_op jit(solution)/shard_map/pallas_call | solution.py:471
  22.7 0.8 %copy.6 = bf16[256,1024]{1,0:T(8,128)(2,1)} copy(bf16[256,1024]{1,0:T(8,128)(2,1)S(1)} %shard_map.46) | data formatting | bytes 1048576

commit v6 on v5

--- a/solution.py
+++ b/solution.py
@@ -272,15 +272,17 @@
         d_s[:, at_b] = (fade * d_s[:, at_b].reshape(rows, e) + total[:, e:]).reshape(MID, chunk, e)
         t_s[:, at_b] = top.reshape(MID, chunk, e)
 
-    def other_planes(m):
+    def far_scores(m):
         q = qp[m].reshape(rows, e)
         k2 = [[kv[i, m, n].reshape(rows, e) for n in range(2)] for i in (0, 2, 1)]
         k_far, v_far = ([cat(*x) for x in zip(*(classes(k2[i][n]) for i in range(3)))] for n in range(2))
         far = [nt(a, b) for a, b in zip(classes(q), k_far)]
-        near_far, own = unclass([x[:, :e] + far_bias[...] for x in far]), unclass([x[:, e:] for x in far])
-        far = near_far
+        far, own = unclass([x[:, :e] + far_bias[...] for x in far]), unclass([x[:, e:] for x in far])
         k_rim, v_rim = (cat(k2[0][n][last * chunk:], k2[1][n][:chunk], outer[n]) for n in range(2))
         rim = nt(cat(q[:chunk], q[last * chunk:]), k_rim) + rim_bias[m]
+        return far, own, rim, v_far, v_rim
+
+    def other_planes(m, far, own, rim, v_far, v_rim):
         peak = jnp.maximum(rim[:, :e], rim[:, e:])
         peak = cat(jnp.maximum(far[:chunk], peak[:chunk]), far[chunk:last * chunk],
                    jnp.maximum(far[last * chunk:], peak[chunk:]))
@@ -328,8 +330,9 @@
 
         if ms[0] == 0:
             find_outer()
-        for m in ms:
-            other_planes(m)
+        scores = [far_scores(m) for m in ms]
+        for m, x in zip(ms, scores):
+            other_planes(m, *x)
         for m in ms:
             for d in range(last):
                 result(m, d).start()
@@ -380,11 +383,15 @@
         arrival(m)
         relay(m, last, True, False)
         relay(m, 0, False, True)
-    for m in range(2, MID):
+    def relay_rest(m):
         for b in range(MID):
             relay(m, b, b != last, b != 0)
+
+    relay_rest(2)
+    pl.when(c == 0)(functools.partial(relay_rest, 3))
     find_ends()
     await_all(qp.at[pl.ds(0, 2), pl.ds(0, last)], ask_r.at[0])
+    pl.when(c == 1)(functools.partial(relay_rest, 3))
     middle(0)
     middle(1)
     await_all(qp.at[pl.ds(0, 2), pl.ds(0, last)], ask_r.at[1])

time: 23.9 us -> 23.6 us (0.987)
  no operation moved by 1% of the time
where the time goes in v6:
time: 23.6 us; the launch traced here: 23.3 us
  Pallas kernels  22.5 us (95%)
  local copies, waits for them, and re-layouts  0.8 us (3%)
    pallas_call x1, Pallas kernels, per_device(): pl.pallas_call(functools.partial(kernel, sp_n, heads), out_shape=pltpu.VM...  22.5 us
    unnamed x1, local copies, waits for them, and re-layouts  0.8 us

profile of v6, /device:TPU:1, one launch (start us, length us, event | category | flops | bytes accessed | tf_op | source)
XLA Modules:
  0.0 23.3 jit_solution(7432913460645958361)
XLA Ops:
  0.0 22.5 %shard_map.46 = bf16[256,1024]{1,0:T(8,128)(2,1)S(1)} custom-call(bf16[256,512]{1,0:T(8,128)(2,1)} %q_hbm.1, bf16[256,512]{1,0:T(8,128)(2,1)} %k_hbm.1, bf16[256,512]{1,0:T(8,128)(2,1)} %v_hbm.1, bf16[1024,1024]{1,0:T(8,128)(2,1)} %w_hbm.1), custom_call_target="tpu_custom_call" | custom-call | tf_op jit(solution)/shard_map/pallas_call | solution.py:478
  22.5 0.8 %copy.6 = bf16[256,1024]{1,0:T(8,128)(2,1)} copy(bf16[256,1024]{1,0:T(8,128)(2,1)S(1)} %shard_map.46) | data formatting | bytes 1048576

commit v7 on v6

--- a/solution.py
+++ b/solution.py
@@ -234,10 +234,13 @@
 
     lane = iota((1, 2 * SIDE), 1)
 
-    def middle(m):
+    def middle_scores(m):
         q = qp[m].reshape(rows, e)
         kh, vh = kv[1, m, 0].reshape(rows, e), kv[1, m, 1].reshape(rows, e)
         mid = cat(*[nt(q[i * half:(i + 1) * half], kh[i * chunk:(i + 3) * chunk]) + mid_bias[i] for i in range(2)])
+        return mid, vh
+
+    def middle(m, mid, vh):
         top = jnp.maximum(jnp.max(mid[:, :e], axis=-1, keepdims=True), jnp.max(mid[:, e:], axis=-1, keepdims=True))
         p_mid = prob(mid, top)
         total = cat(*[nn(p_mid[i * half:(i + 1) * half], with_ones(vh[i * chunk:(i + 3) * chunk])) for i in range(2)])
@@ -392,12 +395,13 @@
     find_ends()
     await_all(qp.at[pl.ds(0, 2), pl.ds(0, last)], ask_r.at[0])
     pl.when(c == 1)(functools.partial(relay_rest, 3))
-    middle(0)
-    middle(1)
+    for m, x in enumerate([middle_scores(0), middle_scores(1)]):
+        middle(m, *x)
     await_all(qp.at[pl.ds(0, 2), pl.ds(0, last)], ask_r.at[1])
-    middle(2)
+    two = [middle_scores(2), middle_scores(3)]
+    middle(2, *two[0])
     scores = near_scores(0)
-    middle(3)
+    middle(3, *two[1])
     for b in range(MID):
         now, scores = scores, near_scores(b + 1) if b < last else None
         near(b, *now)

time: 23.6 us -> 23.6 us (level)
  no operation moved by 1% of the time
where the time goes in v7:
time: 23.6 us; the launch traced here: 23.2 us
  Pallas kernels  22.4 us (95%)
  local copies, waits for them, and re-layouts  0.8 us (3%)
    pallas_call x1, Pallas kernels, per_device(): pl.pallas_call(functools.partial(kernel, sp_n, heads), out_shape=pltpu.VM...  22.4 us
    unnamed x1, local copies, waits for them, and re-layouts  0.8 us

profile of v7, /device:TPU:1, one launch (start us, length us, event | category | flops | bytes accessed | tf_op | source)
XLA Modules:
  0.0 23.2 jit_solution(9172654162558438035)
XLA Ops:
  0.0 22.4 %shard_map.46 = bf16[256,1024]{1,0:T(8,128)(2,1)S(1)} custom-call(bf16[256,512]{1,0:T(8,128)(2,1)} %q_hbm.1, bf16[256,512]{1,0:T(8,128)(2,1)} %k_hbm.1, bf16[256,512]{1,0:T(8,128)(2,1)} %v_hbm.1, bf16[1024,1024]{1,0:T(8,128)(2,1)} %w_hbm.1), custom_call_target="tpu_custom_call" | custom-call | tf_op jit(solution)/shard_map/pallas_call | solution.py:482
  22.4 0.8 %copy.6 = bf16[256,1024]{1,0:T(8,128)(2,1)} copy(bf16[256,1024]{1,0:T(8,128)(2,1)S(1)} %shard_map.46) | data formatting | bytes 1048576
